TPU v7x, 512 devices: a whole 4x8x8 slice. The times are simulated.
512 devices in a mesh: sp: 32 (over z, x), tp: 16 (over y, core).
Axes of the slice: x: 4, y: 8, z: 8, core: 2. Of those that a mesh axis runs over, the one named last changes fastest.
Arguments:
- latent: bfloat16 [16384, 2048], P('sp'), may hold values from -6 to 6
- context: bfloat16 [512, 2048], P('sp'), may hold values from -6 to 6
- condition: bfloat16 [2048], replicated, may hold values from -6 to 6
- context_condition: bfloat16 [2048], replicated, may hold values from -6 to 6
- shift_weight: bfloat16 [2048, 2048], P('sp', 'tp'), may hold values from -0.125 to 0.125
- scale_weight: bfloat16 [2048, 2048], P('sp', 'tp'), may hold values from -0.125 to 0.125
- mod_gate_weight: bfloat16 [2048, 2048], P('sp', 'tp'), may hold values from -0.5 to 0.5
- norm_gain: bfloat16 [2048], replicated, may hold values from 0.099609375 to 1.8984375
- query_weight: bfloat16 [2048, 2048], P(None, 'tp'), may hold values from -0.125 to 0.125
- key_weight: bfloat16 [2048, 2048], P(None, 'tp'), may hold values from -0.125 to 0.125
- value_weight: bfloat16 [2048, 2048], P(None, 'tp'), may hold values from -0.125 to 0.125
- gate_weight: bfloat16 [2048, 2048], P(None, 'tp'), may hold values from -0.125 to 0.125
- forward_decay: float32 [16], P('tp'), may hold values from 0 to 1, as said below
- backward_decay: float32 [16], P('tp'), may hold values from 0 to 1, as said below
- out_weight: bfloat16 [2048, 2048], P('tp'), may hold values from -0.125 to 0.125
Outputs:
- mixed: bfloat16 [16384, 2048], P('sp')
Inputs may be any that keep to these rules, and one draw needn't show every extreme that they name: `forward_decay`: each head's rate is positive. `backward_decay`: each head's rate is positive.
All inputs are finite; a program needn't handle non-finite values.
Results may differ from a plain program's by a relative error of at most 0.015.
Values may be sent and summed in bfloat16 or wider, within the bound.
No kernel may reach another device: no remote copies, remote signals or barrier semaphores. Data moves between devices by JAX's collectives and lax.ppermute only.
A program may use at most 64 MiB of HBM per device.

v0:
```python
import jax
import jax.numpy as jnp
from jax import lax
from jax.sharding import Mesh
from jax.sharding import PartitionSpec as P

HEAD_DIM = 128
GRID_W = 64
SP = ("sp_0", "sp_1")
EPS = 1e-06
THETA = 10000.0
CONTEXT_LIFT = 3.0
TOP_PRECISION = lax.Precision.HIGHEST


def sent_to_all(x, axis):
    copies = jnp.broadcast_to(x, (lax.axis_size(axis), *x.shape))
    return lax.all_to_all(copies, axis, split_axis=0, concat_axis=0, tiled=True)


def taken_together(x, axis):
    everything = sent_to_all(x, axis)
    return jnp.sum(everything, axis=0)


def in_one(arrays, axis):
    ravelled, at, finished = (jnp.concatenate([a.reshape(-1) for a in arrays]), 0, [])
    total = lax.psum(ravelled, axis)
    for a in arrays:
        finished.append(total[at : at + a.size].reshape(a.shape))
        at += a.size
    return tuple(finished)


def filled_with(x, identity):
    return jax.tree.map(
        lambda a, e: jnp.broadcast_to(jnp.asarray(e, a.dtype), a.shape), x, identity
    )


def all_in_one(x, axis):
    leaves = jax.tree.leaves(x)
    order = sorted(range(len(leaves)), key=lambda k: -leaves[k].size)
    width = (1, *leaves[order[0]].shape)[-1]
    lines = [
        jnp.pad(leaves[k].reshape(-1), (0, -leaves[k].size % width)).reshape(-1, width)
        for k in order
    ]
    both, at, found = (lax.all_gather(jnp.concatenate(lines), axis), 0, {})
    for k, line in zip(order, lines):
        slab = both[:, at : at + len(line)].reshape(len(both), -1)
        found[k] = slab[:, : leaves[k].size].reshape(-1, *leaves[k].shape)
        at += len(line)
    numbers = iter(range(len(leaves)))
    return jax.tree.map(lambda _: found[next(numbers)], x)


def prefix_by_axis(x, axes, combine, identity, reverse):
    before = start = filled_with(x, identity)
    total = x
    for axis in reversed(axes):
        length, mine = (lax.axis_size(axis), lax.axis_index(axis))
        pieces = all_in_one(total, axis)
        inside, total = (start, start)
        for k in reversed(range(length)) if reverse else range(length):
            passed = k > mine if reverse else k < mine
            total = combine(total, jax.tree.map(lambda part: part[k], pieces))
            inside = jax.tree.map(lambda new, old: jnp.where(passed, new, old), total, inside)
        before = combine(inside, before)
    return before


def laid_out(parts, dim):
    dims = list(parts.shape[1:])
    dims[dim] *= parts.shape[0]
    return jnp.moveaxis(parts, 0, dim).reshape(dims)


def collect(x, axis, dim):
    return laid_out(sent_to_all(x, axis), dim)


def modulated(token_rows, norm_gain, shifts, scales):
    values = token_rows.astype(jnp.float32)
    values = values * lax.rsqrt(jnp.mean(values * values, axis=-1, keepdims=True) + EPS)
    values = values * norm_gain.astype(jnp.float32)
    return (values * (1.0 + scales) + shifts).astype(jnp.bfloat16)


def rope_half(portion, positions):
    quarter = portion.shape[-1] // 2
    frequency = THETA ** (-jnp.arange(quarter, dtype=jnp.float32) / quarter)
    angles = positions[:, None, None] * frequency
    cosine = jnp.cos(angles)
    sine_table = jnp.sin(angles)
    leading = portion[..., :quarter]
    trailing = portion[..., quarter:]
    return jnp.concatenate(
        [leading * cosine - trailing * sine_table, leading * sine_table + trailing * cosine],
        axis=-1,
    )


def rotate(values, grid_row, grid_column):
    half_width = values.shape[-1] // 2
    return jnp.concatenate(
        [
            rope_half(values[..., :half_width], grid_row),
            rope_half(values[..., half_width:], grid_column),
        ],
        axis=-1,
    )


def combine(earlier, later):
    return (earlier[0] * later[0], later[0][:, None, None] * earlier[1] + later[1])


def local(
    latent,
    context,
    condition,
    context_condition,
    shift_weight,
    scale_weight,
    mod_gate_weight,
    norm_gain,
    query_weight,
    key_weight,
    value_weight,
    gate_weight,
    forward_decay,
    backward_decay,
    out_weight,
):
    sp_index = lax.axis_index(SP)
    tp_index = lax.axis_index("tp")
    sp_count = lax.axis_size(SP)
    tp_count = lax.axis_size("tp")
    tokens_here = latent.shape[0]
    local_rows = tokens_here // tp_count
    mod_rows = shift_weight.shape[0]
    activation = jax.nn.silu(jnp.stack([condition, context_condition]).astype(jnp.float32)).astype(
        jnp.bfloat16
    )
    own_part = lax.dynamic_slice_in_dim(activation, sp_index * mod_rows, mod_rows, 1)
    partial_value = jnp.stack(
        [
            jnp.dot(own_part, matrix, preferred_element_type=jnp.float32)
            for matrix in (shift_weight, scale_weight, mod_gate_weight)
        ]
    )
    summed = taken_together(partial_value, SP)
    modulation = lax.all_gather(summed, "tp", axis=2, tiled=True)
    hidden = modulated(latent, norm_gain, modulation[0, 0], modulation[1, 0])
    context_hidden = modulated(context, norm_gain, modulation[0, 1], modulation[1, 1])
    local_width = query_weight.shape[1]
    head_count = local_width // HEAD_DIM
    stacked = jnp.concatenate([query_weight, key_weight, value_weight, gate_weight], axis=1)
    projected = jnp.dot(hidden, stacked, preferred_element_type=jnp.float32).astype(jnp.bfloat16)
    queries = projected[:, :local_width]
    keys_out = projected[:, local_width : 2 * local_width]
    values_out = projected[:, 2 * local_width : 3 * local_width]
    out_gates = projected[:, 3 * local_width :]
    context_pairs = jnp.dot(
        context_hidden,
        stacked[:, local_width : 3 * local_width],
        preferred_element_type=jnp.float32,
    ).astype(jnp.bfloat16)

    def to_heads(values):
        return values.astype(jnp.float32).reshape(values.shape[0], head_count, HEAD_DIM)

    positions = sp_index * tokens_here + jnp.arange(tokens_here, dtype=jnp.int32)
    grid_row = (positions // GRID_W).astype(jnp.float32)
    grid_column = (positions % GRID_W).astype(jnp.float32)
    key_scale = HEAD_DIM ** (-0.5)
    query_heads = jnp.transpose(rotate(to_heads(queries), grid_row, grid_column), (1, 0, 2))
    key_heads = (
        jnp.transpose(rotate(to_heads(keys_out), grid_row, grid_column), (1, 0, 2)) * key_scale
    )
    value_heads = jnp.transpose(to_heads(values_out), (1, 0, 2))
    log_forward = -forward_decay
    log_backward = -backward_decay
    context_rows = context.shape[0]
    context_total = context_rows * sp_count
    context_index = (sp_index * context_rows + jnp.arange(context_rows, dtype=jnp.int32)).astype(
        jnp.float32
    )
    weight_forward = jnp.exp(log_forward[:, None] * (context_total - 1.0 - context_index)[None, :])
    weight_backward = jnp.exp(log_backward[:, None] * context_index[None, :])
    context_key_heads = to_heads(context_pairs[:, :local_width]) * (key_scale * CONTEXT_LIFT)
    context_value_heads = to_heads(context_pairs[:, local_width:])
    context_forward = jnp.einsum(
        "hc,chd,che->hde",
        weight_forward,
        context_key_heads,
        context_value_heads,
        precision=TOP_PRECISION,
    )
    context_backward = jnp.einsum(
        "hc,chd,che->hde",
        weight_backward,
        context_key_heads,
        context_value_heads,
        precision=TOP_PRECISION,
    )
    context_forward, context_backward = in_one((context_forward, context_backward), SP)
    offsets = jnp.arange(tokens_here, dtype=jnp.float32)
    distance = offsets[:, None] - offsets[None, :]
    mixing = jnp.where(
        distance >= 0, jnp.exp(log_forward[:, None, None] * jnp.maximum(distance, 0.0)), 0.0
    )
    mixing = mixing + jnp.where(
        distance <= 0, jnp.exp(log_backward[:, None, None] * jnp.maximum(-distance, 0.0)), 0.0
    )
    score_matrix = (
        jnp.einsum("htd,hsd->hts", query_heads, key_heads, precision=TOP_PRECISION) * mixing
    )
    local_out = jnp.einsum("hts,hse->hte", score_matrix, value_heads, precision=TOP_PRECISION)
    tail_forward = jnp.exp(log_forward[:, None] * (tokens_here - 1.0 - offsets)[None, :])
    head_backward = jnp.exp(log_backward[:, None] * offsets[None, :])
    own_forward = jnp.einsum(
        "ht,htd,hte->hde", tail_forward, key_heads, value_heads, precision=TOP_PRECISION
    )
    own_backward = jnp.einsum(
        "ht,htd,hte->hde", head_backward, key_heads, value_heads, precision=TOP_PRECISION
    )
    span_forward = jnp.exp(log_forward * tokens_here)
    span_backward = jnp.exp(log_backward * tokens_here)
    identity = (jnp.ones_like(span_forward), jnp.zeros_like(own_forward))
    before = prefix_by_axis((span_forward, own_forward), SP, combine, identity, False)
    after = prefix_by_axis((span_backward, own_backward), SP, combine, identity, True)
    device_start = (sp_index * tokens_here).astype(jnp.float32)
    device_rest = ((sp_count - 1 - sp_index) * tokens_here).astype(jnp.float32)
    incoming_forward = (
        before[1] + jnp.exp(log_forward * device_start)[:, None, None] * context_forward
    )
    incoming_backward = (
        after[1] + jnp.exp(log_backward * device_rest)[:, None, None] * context_backward
    )
    read_forward = jnp.exp(log_forward[:, None] * (offsets + 1.0)[None, :])[
        :, :, None
    ] * jnp.einsum("htd,hde->hte", query_heads, incoming_forward, precision=TOP_PRECISION)
    read_backward = jnp.exp(log_backward[:, None] * (tokens_here - offsets)[None, :])[
        :, :, None
    ] * jnp.einsum("htd,hde->hte", query_heads, incoming_backward, precision=TOP_PRECISION)
    retained = local_out + read_forward + read_backward
    retained = retained * lax.rsqrt(jnp.mean(retained * retained, axis=-1, keepdims=True) + EPS)
    merged = jnp.transpose(retained, (1, 0, 2)).reshape(tokens_here, local_width)
    heads_out = (jax.nn.silu(out_gates.astype(jnp.float32)) * merged).astype(jnp.bfloat16)
    projection = lax.psum_scatter(
        jnp.dot(heads_out, out_weight, preferred_element_type=jnp.float32),
        "tp",
        scatter_dimension=0,
        tiled=True,
    )
    own_latent = lax.dynamic_slice_in_dim(latent, tp_index * local_rows, local_rows, 0)
    finished = (own_latent.astype(jnp.float32) + modulation[2, 0] * projection).astype(jnp.bfloat16)
    return collect(finished, "tp", 0)


def solution(mesh):
    torus = Mesh(mesh.devices.reshape(8, 4, mesh.shape["tp"]), ("sp_0", "sp_1", "tp"))
    in_specs = (
        P(SP, None),
        P(SP, None),
        P(),
        P(),
        P(SP, "tp"),
        P(SP, "tp"),
        P(SP, "tp"),
        P(),
        P(None, "tp"),
        P(None, "tp"),
        P(None, "tp"),
        P(None, "tp"),
        P("tp"),
        P("tp"),
        P("tp", None),
    )
    out_specs = P(SP, None)
    return jax.shard_map(local, mesh=torus, in_specs=in_specs, out_specs=out_specs, check_vma=False)
```

profile of v0, /device:TPU:1, one launch (start us, length us, event | category | flops | bytes accessed | tf_op | source)
XLA Modules:
  0.0 352.9 jit_solution(17837896909596042663)
XLA Ops:
  6.5 0.8 stack.21
  7.4 0.7 stack.22
  8.1 0.9 convolution_bitcast_fusion.4
  9.0 0.9 convolution_bitcast_fusion.3
  9.9 0.9 convolution_bitcast_fusion.2
  10.9 0.7 broadcast_in_dim.10
  11.5 13.7 %all-to-all-start = ((f32[32,3,2,128]{3,2,1,0:T(2,128)}), f32[32,3,2,128]{3,2,1,0:T(2,128)S(1)}, u32[]{:S(2)}, u32[]{:S(2)}) async-start(f32[32,3,2,128]{3,2,1,0:T(2,128)} %broadcast_in_dim.10), calls=%async_computation | async-start | bytes 196608 | tf_op jit(solution)/shard_map/all_to_all | solution.py:18
  27.0 1.0 fusion.45
  28.0 2.1 fusion
  30.0 0.7 convert_element_type.83
  30.7 3.6 %all-to-all-done = f32[32,3,2,128]{3,2,1,0:T(2,128)S(1)} async-done(((f32[32,3,2,128]{3,2,1,0:T(2,128)}), f32[32,3,2,128]{3,2,1,0:T(2,128)S(1)}, u32[]{:S(2)}, u32[]{:S(2)}) %all-to-all-start) | async-done | bytes 98336 | tf_op jit(solution)/shard_map/all_to_all | solution.py:18
  34.4 19.6 %all_gather.27 = f32[3,2,2048]{2,1,0:T(2,128)S(1)} all-gather(f32[3,2,128]{2,1,0:T(2,128)S(1)} %reduce_sum.36), channel_id=1, replica_groups=mesh['sp_0'=8,'sp_1'=4,'tp'=16] {'tp'}, dimensions={2}, use_global_device_ids=true | all-gather | bytes 52224 | tf_op jit(solution)/shard_map/all_gather | solution.py:154
  54.1 1.5 convolution_convert_fusion
  57.0 2.9 fusion.18
  61.1 9.4 %all-gather.4 = f32[4,129,128]{2,1,0:T(8,128)S(1)} all-gather(f32[1,129,128]{2,1,0:T(8,128)S(1)} %maximum_bitcast_fusion.4), channel_id=2, replica_groups=mesh['sp_0'=8,'sp_1'=4,'tp'=16] {'sp_1'}, dimensions={0}, use_global_device_ids=true | all-gather | bytes 330240 | tf_op jit(solution)/shard_map/all_gather | solution.py:49
  74.4 9.7 %all-gather.6 = f32[4,129,128]{2,1,0:T(8,128)S(1)} all-gather(f32[1,129,128]{2,1,0:T(8,128)S(1)} %maximum_bitcast_fusion.6), channel_id=4, replica_groups=mesh['sp_0'=8,'sp_1'=4,'tp'=16] {'sp_1'}, dimensions={0}, use_global_device_ids=true | all-gather | bytes 330240 | tf_op jit(solution)/shard_map/all_gather | solution.py:49
  89.2 2.0 fusion.233
  91.1 19.6 %all-gather.7 = f32[8,129,128]{2,1,0:T(8,128)S(1)} all-gather(f32[1,129,128]{2,1,0:T(8,128)S(1)} %maximum_bitcast_fusion.7), channel_id=5, replica_groups=mesh['sp_0'=8,'sp_1'=4,'tp'=16] {'sp_0'}, dimensions={0}, use_global_device_ids=true | all-gather | bytes 594432 | tf_op jit(solution)/shard_map/all_gather | solution.py:49
  110.7 0.7 fusion.224
  111.4 1.9 fusion.234
  113.3 20.3 %all-gather.5 = f32[8,129,128]{2,1,0:T(8,128)S(1)} all-gather(f32[1,129,128]{2,1,0:T(8,128)S(1)} %maximum_bitcast_fusion.5), channel_id=3, replica_groups=mesh['sp_0'=8,'sp_1'=4,'tp'=16] {'sp_0'}, dimensions={0}, use_global_device_ids=true | all-gather | bytes 594432 | tf_op jit(solution)/shard_map/all_gather | solution.py:49
  133.7 0.7 fusion.225
  135.6 1.5 convolution_multiply_fusion
  137.2 0.7 fusion.62
  137.9 61.9 %all-reduce.6.cloned.1.call-done = f32[32768]{0:T(1024)} async-done(((f32[32768]{0:T(1024)}), f32[32768]{0:T(1024)}) %all-reduce.6.cloned.1.call-update) | async-done | bytes 131088 | tf_op jit(solution)/shard_map/psum | solution.py:28
  199.9 8.0 %fusion.24 = f32[512,128]{0,1:T(8,128)S(1)} fusion(f32[512,128]{0,1:T(8,128)S(1)} %fusion.62, f32[512]{0:T(512)S(1)} %multiply_exponential_fusion.1, f32[32768]{0:T(1024)} %all-reduce.6.cloned.1.call-done, f32[8,129,128]{2,1,0:T(8,128)} %copy-done.3, f32[4,129,128]{2,1,0:T(8,128)S(1)} %all-gather.4, f32[512,1,32]{0,2,1:T(8,128)} %copy-done.5, ...), kind=kOutput, calls=%fused_computation.26 | convolution fusion | flops 101695488 | bytes 1847816 | tf_op jit(solution)/shard_map/htd,hde->hte/dot_general | solution.py:244
  207.9 8.0 %multiply_reduce_fusion = (f32[512]{0:T(512)S(1)}, f32[512,128]{0,1:T(8,128)S(1)}) fusion(f32[512,128]{0,1:T(8,128)S(1)} %fusion.24, f32[32768]{0:T(1024)} %all-reduce.6.cloned.1.call-done, f32[8,129,128]{2,1,0:T(8,128)} %copy-done.2, f32[4,129,128]{2,1,0:T(8,128)S(1)} %all-gather.6, f32[]{:T(128)} %bitcast.75, f32[]{:T(128)} %bitcast.76, f32[]{:T(128)} %bitcast.77, ...), kind=kOutput, calls=%fused_computation.53 | convolution fusion | flops 101826048 | bytes 1849864 | tf_op jit(solution)/shard_map/htd,hde->hte/dot_general | solution.py:247
  215.9 3.6 %fusion.50 = f32[512,2048]{1,0:T(8,128)} fusion(bf16[128,2048]{1,0:T(8,128)(2,1)S(1)} %copy-done, f32[512,128]{0,1:T(8,128)S(1)} %get-tuple-element.53, bf16[512,512]{0,1:T(8,128)(2,1)} %copy-done.4, f32[512]{0:T(512)S(1)} %add_rsqrt_fusion), kind=kOutput, calls=%fused_computation.66 | convolution fusion | flops 268959744 | bytes 5113856 | tf_op jit(solution)/shard_map/dot_general | solution.py:253
  219.5 66.3 %reduce-scatter.2.cloned.1.call-done = f32[32,2048]{1,0:T(8,128)} async-done(((f32[512,2048]{1,0:T(8,128)}), f32[32,2048]{1,0:T(8,128)}) %reduce-scatter.2.cloned.1.call-update) | async-done | bytes 262160 | tf_op jit(solution)/shard_map/reduce_scatter | solution.py:252
  285.8 1.0 add_convert_fusion
  287.1 57.7 %all_to_all.10 = bf16[16,32,2048]{2,1,0:T(8,128)(2,1)S(1)} all-to-all(bf16[16,32,2048]{2,1,0:T(8,128)(2,1)S(1)} %broadcast_in_dim.12), channel_id=1, replica_groups=mesh['sp_0'=8,'sp_1'=4,'tp'=16] {'tp'}, dimensions={0} | all-to-all | bytes 4194304 | tf_op jit(solution)/shard_map/all_to_all | solution.py:18
  344.8 1.3 copy.34
  (58 shorter events, 4.3 us)
Async XLA Ops:
  6.5 209.4 %copy-start = (bf16[128,2048]{1,0:T(8,128)(2,1)S(1)}, bf16[128,2048]{1,0:T(8,128)(2,1)}, u32[]{:S(2)}) copy-start(bf16[128,2048]{1,0:T(8,128)(2,1)} %param.29) | copy-start | bytes 1572868
  6.5 50.4 %copy-start.1 = (bf16[512,2048]{1,0:T(8,128)(2,1)S(1)}, bf16[512,2048]{1,0:T(8,128)(2,1)}, u32[]{:S(2)}) copy-start(bf16[512,2048]{1,0:T(8,128)(2,1)} %param.15) | copy-start | bytes 6291460
  6.5 50.4 %copy-start.8 = (bf16[2048,128]{1,0:T(8,128)(2,1)S(1)}, bf16[2048,128]{1,0:T(8,128)(2,1)}, u32[]{:S(2)}) copy-start(bf16[2048,128]{1,0:T(8,128)(2,1)} %param.25) | copy-start | bytes 1572868
  11.5 22.8 %all-to-all-start = ((f32[32,3,2,128]{3,2,1,0:T(2,128)}), f32[32,3,2,128]{3,2,1,0:T(2,128)S(1)}, u32[]{:S(2)}, u32[]{:S(2)}) async-start(f32[32,3,2,128]{3,2,1,0:T(2,128)} %broadcast_in_dim.10), calls=%async_computation | async-start | bytes 196608 | tf_op jit(solution)/shard_map/all_to_all | solution.py:18
  25.3 174.6 %all-reduce.6.cloned.1.call-start = ((), (), s32[]{:S(2)}) async-start(), calls=%async_computation.3 | async-start | bytes 262144 | tf_op jit(solution)/shard_map/psum | solution.py:28
  56.9 228.9 %reduce-scatter.2.cloned.1.call-start = ((), (), s32[]{:S(2)}) async-start(), calls=%async_computation.4 | async-start | bytes 4456448 | tf_op jit(solution)/shard_map/reduce_scatter | solution.py:252
  59.9 77.3 %copy-start.4 = (bf16[512,512]{0,1:T(8,128)(2,1)}, bf16[512,512]{0,1:T(8,128)(2,1)S(1)}, u32[]{:S(2)}) copy-start(bf16[512,512]{0,1:T(8,128)(2,1)S(1)} %fusion.18) | copy-start | bytes 1572868
  60.5 76.6 %copy-start.5 = (f32[512,1,32]{0,2,1:T(8,128)}, f32[512,1,32]{0,2,1:T(8,128)S(1)}, u32[]{:S(2)}) copy-start(f32[512,1,32]{0,2,1:T(8,128)S(1)} %get-tuple-element.25) | copy-start | bytes 196612
  60.5 76.6 %copy-start.6 = (f32[512,1,32]{0,2,1:T(8,128)}, f32[512,1,32]{0,2,1:T(8,128)S(1)}, u32[]{:S(2)}) copy-start(f32[512,1,32]{0,2,1:T(8,128)S(1)} %get-tuple-element.26) | copy-start | bytes 196612
  60.6 76.6 %copy-start.7 = (f32[512,1,32]{0,2,1:T(8,128)}, f32[512,1,32]{0,2,1:T(8,128)S(1)}, u32[]{:S(2)}) copy-start(f32[512,1,32]{0,2,1:T(8,128)S(1)} %get-tuple-element.27) | copy-start | bytes 196612
  110.7 24.9 %copy-start.2 = (f32[8,129,128]{2,1,0:T(8,128)}, f32[8,129,128]{2,1,0:T(8,128)S(1)}, u32[]{:S(2)}) copy-start(f32[8,129,128]{2,1,0:T(8,128)S(1)} %all-gather.7) | copy-start | bytes 1585156
  133.7 2.0 copy-start.3
Sparse Core Ops, SparseCore 0:
  57.0 142.7 all-reduce.5
  219.6 66.1 reduce-scatter.1
where the time goes:
time: 354 us; the launch traced here: 353 us
  blocking collectives  136 us (38%)
  waiting for transfers between devices  132 us (37%)
  matrix products  30.2 us (9%)
  between operations  24.2 us (7%)
  starting transfers between devices  13.8 us (4%)
  other arithmetic  10.1 us (3%)
  local copies, waits for them, and re-layouts  6.43 us (2%)
    reduce_scatter x1, waiting for transfers between devices, local(): lax.psum_scatter(jnp.dot(heads_out, out_weight, preferred_element_type=jn...  66.3 us
    psum x1, waiting for transfers between devices, in_one(): total = lax.psum(ravelled, axis)  61.9 us
    all_gather x4, blocking collectives, all_in_one(): both, at, found = (lax.all_gather(jnp.concatenate(lines), axis), 0, {})  59 us
    all_to_all x1, blocking collectives, sent_to_all(): return lax.all_to_all(copies, axis, split_axis=0, concat_axis=0, tiled=True)  57.7 us
    all_gather x1, blocking collectives, local(): modulation = lax.all_gather(summed, 'tp', axis=2, tiled=True)  19.6 us
    all_to_all x1, starting transfers between devices, sent_to_all(): return lax.all_to_all(copies, axis, split_axis=0, concat_axis=0, tiled=True)  13.7 us
    dot_general x1, matrix products, local(): jnp.einsum('htd,hde->hte', query_heads, incoming_forward, precision=TOP_P...  8.03 us
    dot_general x1, matrix products, local(): jnp.einsum('htd,hde->hte', query_heads, incoming_backward, precision=TOP_...  7.98 us
  transfers between devices with their start and end apart: 3, of which 3 were waited for; matrix products, arithmetic and copies ran while one was open for 5% of the time, Pallas kernels for 0%

commit v1 on v0

--- a/solution.py
+++ b/solution.py
@@ -151,7 +151,9 @@
         ]
     )
     summed = taken_together(partial_value, SP)
-    modulation = lax.all_gather(summed, "tp", axis=2, tiled=True)
+    modulation = jnp.concatenate(
+        lax.all_to_all(jnp.stack([summed] * lax.axis_size("tp")), "tp", 0, 0), axis=2
+    )
     hidden = modulated(latent, norm_gain, modulation[0, 0], modulation[1, 0])
     context_hidden = modulated(context, norm_gain, modulation[0, 1], modulation[1, 1])
     local_width = query_weight.shape[1]

time: 354 us -> 350 us (0.989)
  blocking collectives: 136 us -> 117 us
  starting transfers between devices: 13.8 us -> 23 us
  waiting for transfers between devices: 132 us -> 137 us
    all_gather x1 -> x0, blocking collectives: 19.6 us -> none  [local(): modulation = lax.all_gather(summed, 'tp', axis=2, tiled=True)]
    all_to_all x0 -> x1, starting transfers between devices: none -> 9.18 us  [local(): lax.all_to_all(jnp.stack([summed] * lax.axis_size('tp')), 'tp', 0, 0)]
    all_to_all x0 -> x1, waiting for transfers between devices: none -> 7.42 us  [local(): lax.all_to_all(jnp.stack([summed] * lax.axis_size('tp')), 'tp', 0, 0)]
  transfers between devices with their start and end apart: 3 -> 4, of which waited for: 3 -> 4; matrix products, arithmetic and copies ran while one was open for 5% -> 5% of each run, Pallas kernels for 0% -> 0%
where the time goes in v1:
time: 350 us; the launch traced here: 348 us
  waiting for transfers between devices  137 us (39%)
  blocking collectives  117 us (33%)
  matrix products  30.1 us (9%)
  between operations  24 us (7%)
  starting transfers between devices  23 us (7%)
  other arithmetic  10.1 us (3%)
  local copies, waits for them, and re-layouts  7.13 us (2%)
    reduce_scatter x1, waiting for transfers between devices, local(): lax.psum_scatter(jnp.dot(heads_out, out_weight, preferred_element_type=jn...  66.1 us
    all_gather x4, blocking collectives, all_in_one(): both, at, found = (lax.all_gather(jnp.concatenate(lines), axis), 0, {})  59.7 us
    psum x1, waiting for transfers between devices, in_one(): total = lax.psum(ravelled, axis)  59.5 us
    all_to_all x1, blocking collectives, sent_to_all(): return lax.all_to_all(copies, axis, split_axis=0, concat_axis=0, tiled=True)  57.6 us
    all_to_all x1, starting transfers between devices, sent_to_all(): return lax.all_to_all(copies, axis, split_axis=0, concat_axis=0, tiled=True)  13.7 us
    all_to_all x1, starting transfers between devices, local(): lax.all_to_all(jnp.stack([summed] * lax.axis_size('tp')), 'tp', 0, 0)  9.18 us
    dot_general x1, matrix products, local(): jnp.einsum('htd,hde->hte', query_heads, incoming_backward, precision=TOP_...  7.94 us
    dot_general x1, matrix products, local(): jnp.einsum('htd,hde->hte', query_heads, incoming_forward, precision=TOP_P...  7.92 us
  transfers between devices with their start and end apart: 4, of which 4 were waited for; matrix products, arithmetic and copies ran while one was open for 5% of the time, Pallas kernels for 0%

profile of v1, /device:TPU:1, one launch (start us, length us, event | category | flops | bytes accessed | tf_op | source)
XLA Modules:
  0.0 348.4 jit_solution(16608590982152766541)
XLA Ops:
  6.5 0.8 stack.16
  7.4 0.7 stack.17
  8.1 0.9 convolution_bitcast_fusion.4
  9.0 0.9 convolution_bitcast_fusion.3
  9.9 0.9 convolution_bitcast_fusion.2
  11.5 13.7 %all-to-all-start = ((f32[32,3,2,128]{3,2,1,0:T(2,128)}), f32[32,3,2,128]{3,2,1,0:T(2,128)S(1)}, u32[]{:S(2)}, u32[]{:S(2)}) async-start(f32[32,3,2,128]{3,2,1,0:T(2,128)} %broadcast_in_dim.10), calls=%async_computation | async-start | bytes 196608 | tf_op jit(solution)/shard_map/all_to_all | solution.py:18
  26.9 1.0 fusion.45
  27.9 2.1 fusion
  30.0 0.7 convert_element_type.83
  30.7 3.7 %all-to-all-done = f32[32,3,2,128]{3,2,1,0:T(2,128)S(1)} async-done(((f32[32,3,2,128]{3,2,1,0:T(2,128)}), f32[32,3,2,128]{3,2,1,0:T(2,128)S(1)}, u32[]{:S(2)}, u32[]{:S(2)}) %all-to-all-start) | async-done | bytes 98336 | tf_op jit(solution)/shard_map/all_to_all | solution.py:18
  35.1 9.2 %all-to-all-start.1 = ((f32[16,3,2,128]{3,2,1,0:T(2,128)}), f32[16,3,2,128]{3,2,1,0:T(2,128)S(1)}, u32[]{:S(2)}, u32[]{:S(2)}) async-start(f32[16,3,2,128]{3,2,1,0:T(2,128)} %stack.23), calls=%async_computation.1 | async-start | bytes 98304 | tf_op jit(solution)/shard_map/all_to_all | solution.py:155
  44.3 7.4 %all-to-all-done.1 = f32[16,3,2,128]{3,2,1,0:T(2,128)S(1)} async-done(((f32[16,3,2,128]{3,2,1,0:T(2,128)}), f32[16,3,2,128]{3,2,1,0:T(2,128)S(1)}, u32[]{:S(2)}, u32[]{:S(2)}) %all-to-all-start.1) | async-done | bytes 49184 | tf_op jit(solution)/shard_map/all_to_all | solution.py:155
  51.8 1.5 convolution_convert_fusion
  54.7 2.9 fusion.18
  58.9 9.7 %all-gather.4 = f32[4,129,128]{2,1,0:T(8,128)S(1)} all-gather(f32[1,129,128]{2,1,0:T(8,128)S(1)} %maximum_bitcast_fusion.4), channel_id=2, replica_groups=mesh['sp_0'=8,'sp_1'=4,'tp'=16] {'sp_1'}, dimensions={0}, use_global_device_ids=true | all-gather | bytes 330240 | tf_op jit(solution)/shard_map/all_gather | solution.py:49
  72.4 10.4 %all-gather.6 = f32[4,129,128]{2,1,0:T(8,128)S(1)} all-gather(f32[1,129,128]{2,1,0:T(8,128)S(1)} %maximum_bitcast_fusion.6), channel_id=4, replica_groups=mesh['sp_0'=8,'sp_1'=4,'tp'=16] {'sp_1'}, dimensions={0}, use_global_device_ids=true | all-gather | bytes 330240 | tf_op jit(solution)/shard_map/all_gather | solution.py:49
  87.7 2.0 fusion.233
  89.7 19.8 %all-gather.7 = f32[8,129,128]{2,1,0:T(8,128)S(1)} all-gather(f32[1,129,128]{2,1,0:T(8,128)S(1)} %maximum_bitcast_fusion.7), channel_id=5, replica_groups=mesh['sp_0'=8,'sp_1'=4,'tp'=16] {'sp_0'}, dimensions={0}, use_global_device_ids=true | all-gather | bytes 594432 | tf_op jit(solution)/shard_map/all_gather | solution.py:49
  109.5 0.7 fusion.224
  110.2 1.9 fusion.234
  112.1 19.8 %all-gather.5 = f32[8,129,128]{2,1,0:T(8,128)S(1)} all-gather(f32[1,129,128]{2,1,0:T(8,128)S(1)} %maximum_bitcast_fusion.5), channel_id=3, replica_groups=mesh['sp_0'=8,'sp_1'=4,'tp'=16] {'sp_0'}, dimensions={0}, use_global_device_ids=true | all-gather | bytes 594432 | tf_op jit(solution)/shard_map/all_gather | solution.py:49
  131.9 0.7 fusion.225
  133.8 1.5 convolution_multiply_fusion
  135.4 0.7 fusion.62
  136.1 59.5 %all-reduce.6.cloned.1.call-done = f32[32768]{0:T(1024)} async-done(((f32[32768]{0:T(1024)}), f32[32768]{0:T(1024)}) %all-reduce.6.cloned.1.call-update) | async-done | bytes 131088 | tf_op jit(solution)/shard_map/psum | solution.py:28
  195.7 7.9 %fusion.24 = f32[512,128]{0,1:T(8,128)S(1)} fusion(f32[512,128]{0,1:T(8,128)S(1)} %fusion.62, f32[512]{0:T(512)S(1)} %multiply_exponential_fusion.1, f32[32768]{0:T(1024)} %all-reduce.6.cloned.1.call-done, f32[8,129,128]{2,1,0:T(8,128)} %copy-done.3, f32[4,129,128]{2,1,0:T(8,128)S(1)} %all-gather.4, f32[512,1,32]{0,2,1:T(8,128)} %copy-done.5, ...), kind=kOutput, calls=%fused_computation.26 | convolution fusion | flops 101695488 | bytes 1847816 | tf_op jit(solution)/shard_map/htd,hde->hte/dot_general | solution.py:246
  203.6 7.9 %multiply_reduce_fusion = (f32[512]{0:T(512)S(1)}, f32[512,128]{0,1:T(8,128)S(1)}) fusion(f32[512,128]{0,1:T(8,128)S(1)} %fusion.24, f32[32768]{0:T(1024)} %all-reduce.6.cloned.1.call-done, f32[8,129,128]{2,1,0:T(8,128)} %copy-done.2, f32[4,129,128]{2,1,0:T(8,128)S(1)} %all-gather.6, f32[]{:T(128)} %bitcast.76, f32[]{:T(128)} %bitcast.77, f32[]{:T(128)} %bitcast.78, ...), kind=kOutput, calls=%fused_computation.53 | convolution fusion | flops 101826048 | bytes 1849864 | tf_op jit(solution)/shard_map/htd,hde->hte/dot_general | solution.py:249
  211.6 3.6 %fusion.50 = f32[512,2048]{1,0:T(8,128)} fusion(bf16[128,2048]{1,0:T(8,128)(2,1)S(1)} %copy-done, f32[512,128]{0,1:T(8,128)S(1)} %get-tuple-element.53, bf16[512,512]{0,1:T(8,128)(2,1)} %copy-done.4, f32[512]{0:T(512)S(1)} %add_rsqrt_fusion), kind=kOutput, calls=%fused_computation.66 | convolution fusion | flops 268959744 | bytes 5113856 | tf_op jit(solution)/shard_map/dot_general | solution.py:255
  215.2 66.1 %reduce-scatter.2.cloned.1.call-done = f32[32,2048]{1,0:T(8,128)} async-done(((f32[512,2048]{1,0:T(8,128)}), f32[32,2048]{1,0:T(8,128)}) %reduce-scatter.2.cloned.1.call-update) | async-done | bytes 262160 | tf_op jit(solution)/shard_map/reduce_scatter | solution.py:254
  281.4 1.0 add_convert_fusion
  282.6 57.6 %all_to_all.15 = bf16[16,32,2048]{2,1,0:T(8,128)(2,1)S(1)} all-to-all(bf16[16,32,2048]{2,1,0:T(8,128)(2,1)S(1)} %broadcast_in_dim.12), channel_id=1, replica_groups=mesh['sp_0'=8,'sp_1'=4,'tp'=16] {'tp'}, dimensions={0} | all-to-all | bytes 4194304 | tf_op jit(solution)/shard_map/all_to_all | solution.py:18
  340.2 1.3 copy.47
  (61 shorter events, 5.7 us)
Async XLA Ops:
  6.5 205.0 %copy-start = (bf16[128,2048]{1,0:T(8,128)(2,1)S(1)}, bf16[128,2048]{1,0:T(8,128)(2,1)}, u32[]{:S(2)}) copy-start(bf16[128,2048]{1,0:T(8,128)(2,1)} %param.29) | copy-start | bytes 1572868
  6.5 48.2 %copy-start.1 = (bf16[512,2048]{1,0:T(8,128)(2,1)S(1)}, bf16[512,2048]{1,0:T(8,128)(2,1)}, u32[]{:S(2)}) copy-start(bf16[512,2048]{1,0:T(8,128)(2,1)} %param.15) | copy-start | bytes 6291460
  6.5 48.2 %copy-start.8 = (bf16[2048,128]{1,0:T(8,128)(2,1)S(1)}, bf16[2048,128]{1,0:T(8,128)(2,1)}, u32[]{:S(2)}) copy-start(bf16[2048,128]{1,0:T(8,128)(2,1)} %param.25) | copy-start | bytes 1572868
  11.5 22.8 %all-to-all-start = ((f32[32,3,2,128]{3,2,1,0:T(2,128)}), f32[32,3,2,128]{3,2,1,0:T(2,128)S(1)}, u32[]{:S(2)}, u32[]{:S(2)}) async-start(f32[32,3,2,128]{3,2,1,0:T(2,128)} %broadcast_in_dim.10), calls=%async_computation | async-start | bytes 196608 | tf_op jit(solution)/shard_map/all_to_all | solution.py:18
  35.1 16.7 %all-to-all-start.1 = ((f32[16,3,2,128]{3,2,1,0:T(2,128)}), f32[16,3,2,128]{3,2,1,0:T(2,128)S(1)}, u32[]{:S(2)}, u32[]{:S(2)}) async-start(f32[16,3,2,128]{3,2,1,0:T(2,128)} %stack.23), calls=%async_computation.1 | async-start | bytes 98304 | tf_op jit(solution)/shard_map/all_to_all | solution.py:155
  44.3 151.4 %all-reduce.6.cloned.1.call-start = ((), (), s32[]{:S(2)}) async-start(), calls=%async_computation.4 | async-start | bytes 262144 | tf_op jit(solution)/shard_map/psum | solution.py:28
  54.7 226.7 %reduce-scatter.2.cloned.1.call-start = ((), (), s32[]{:S(2)}) async-start(), calls=%async_computation.5 | async-start | bytes 4456448 | tf_op jit(solution)/shard_map/reduce_scatter | solution.py:254
  57.6 77.8 %copy-start.4 = (bf16[512,512]{0,1:T(8,128)(2,1)}, bf16[512,512]{0,1:T(8,128)(2,1)S(1)}, u32[]{:S(2)}) copy-start(bf16[512,512]{0,1:T(8,128)(2,1)S(1)} %fusion.18) | copy-start | bytes 1572868
  58.3 77.1 %copy-start.5 = (f32[512,1,32]{0,2,1:T(8,128)}, f32[512,1,32]{0,2,1:T(8,128)S(1)}, u32[]{:S(2)}) copy-start(f32[512,1,32]{0,2,1:T(8,128)S(1)} %get-tuple-element.25) | copy-start | bytes 196612
  58.3 77.1 %copy-start.6 = (f32[512,1,32]{0,2,1:T(8,128)}, f32[512,1,32]{0,2,1:T(8,128)S(1)}, u32[]{:S(2)}) copy-start(f32[512,1,32]{0,2,1:T(8,128)S(1)} %get-tuple-element.26) | copy-start | bytes 196612
  58.3 77.1 %copy-start.7 = (f32[512,1,32]{0,2,1:T(8,128)}, f32[512,1,32]{0,2,1:T(8,128)S(1)}, u32[]{:S(2)}) copy-start(f32[512,1,32]{0,2,1:T(8,128)S(1)} %get-tuple-element.27) | copy-start | bytes 196612
  109.5 24.3 %copy-start.2 = (f32[8,129,128]{2,1,0:T(8,128)}, f32[8,129,128]{2,1,0:T(8,128)S(1)}, u32[]{:S(2)}) copy-start(f32[8,129,128]{2,1,0:T(8,128)S(1)} %all-gather.7) | copy-start | bytes 1585156
  131.9 2.0 copy-start.3
Sparse Core Ops, SparseCore 0:
  54.8 140.8 all-reduce.5
  215.3 65.9 reduce-scatter.1
